TPU v7x, 512 devices: a whole 4x4x16 slice. The times are simulated.
512 devices in a mesh: ep: 32 (over z, core), tp: 16 (over y, x).
Axes of the slice: x: 4, y: 4, z: 16, core: 2. Of those that a mesh axis runs over, the one named last changes fastest.
Arguments:
- mixer_input: bfloat16 [8192, 2048], P('ep'), may hold values from -6 to 6
- mixer_gain: float32 [2048], replicated, may hold values from 0.1 to 1.9
- query_weight: bfloat16 [2048, 2048], P(None, 'tp'), may hold values from -0.13258252 to 0.13258252
- key_weight: bfloat16 [2048, 1024], P(None, 'tp'), may hold values from -2.78423295 to 2.78423295
- value_weight: bfloat16 [2048, 1024], P(None, 'tp'), may hold values from -0.125 to 0.125
- output_weight: bfloat16 [2048, 2048], P(None, 'tp'), may hold values from -1 to 1
- sink_logit: float32 [32], P('tp'), may hold values from 2 to 7
- expert_input: bfloat16 [4096, 2048], P('ep'), may hold values from -6 to 6
- expert_gain: float32 [2048], replicated, may hold values from 0.1 to 1.9
- routes: int32 [4096, 4], P('ep'), may hold values from 0 to 31, all different within a row; in each aligned block of 128 rows (0 to 127, 128 to 255, ...) at most 32 rows name the same one
- route_logits: float32 [4096, 4], P('ep'), may hold values from -6 to 6
- gate_weight: bfloat16 [32, 2048, 2048], P('ep', None, 'tp'), may hold values from -0.375 to 0.375
- up_weight: bfloat16 [32, 2048, 2048], P('ep', None, 'tp'), may hold values from -0.375 to 0.375
- down_weight: bfloat16 [32, 2048, 2048], P('ep', None, 'tp'), may hold values from -0.03125 to 0.03125
Outputs:
- mixer_output: bfloat16 [8192, 2048], P('ep', 'tp')
- expert_output: bfloat16 [4096, 2048], P('ep', 'tp')
Inputs may be any that keep to these rules, and one draw needn't show every extreme that they name: `routes`: each token names 4 different experts. Among the 128 tokens of one index of ep (aligned blocks) no expert is named more than 32 times, and in some blocks one expert is named exactly 32 times.
All inputs are finite; a program needn't handle non-finite values.
Results may differ from a plain program's by a relative error of at most 0.0055.
The roundings to bfloat16 on the way count: a program that leaves them out, or rounds other values in their place, can miss the bound.
Values may be sent and summed in bfloat16 or wider, within the bound.
No kernel may reach another device: no remote copies, remote signals or barrier semaphores. Data moves between devices by JAX's collectives and lax.ppermute only.
A program may use at most 64 MiB of HBM per device.

v0:
```python
import jax
import jax.numpy as jnp
from jax import lax
from jax.sharding import Mesh
from jax.sharding import PartitionSpec as P

HEAD_DIM = 64
TOP_K = 4
WINDOW = 128
GRID_W = 64
EP = ("ep_0", "ep_1")
EPSILON = 1e-06
LIMIT = 7.0
SLOPE = 1.702
BASE = 10000.0


def extended(shard, sides, width):
    for axis, dim in sides:
        devices, length = (lax.axis_size(axis), shard.shape[dim])
        up = [(i, (i + 1) % devices) for i in range(devices - 1)]
        down = [(j, i) for i, j in up]
        last = lax.slice_in_dim(shard, length - width, length, axis=dim)
        first = lax.slice_in_dim(shard, 0, width, axis=dim)
        before = lax.ppermute(last, axis, up)
        after = lax.ppermute(first, axis, down)
        shard = jnp.concatenate([before, shard, after], axis=dim)
    return shard


def cut_along(shard, dim, devices):
    shape = shard.shape
    pieces = shard.reshape(*shape[:dim], devices, shape[dim] // devices, *shape[dim + 1 :])
    return jnp.moveaxis(pieces, dim, 0)


def joined_along(pieces, dim):
    pieces = jnp.moveaxis(pieces, 0, dim)
    shape = pieces.shape
    return pieces.reshape(*shape[:dim], shape[dim] * shape[dim + 1], *shape[dim + 2 :])


def exchange_in_order(pieces, axes, order):
    inside = pieces.shape[1:]
    whole = pieces.reshape(*(lax.axis_size(a) for a in axes), *inside)
    for k in order:
        whole = lax.all_to_all(whole, axes[k], k, k, tiled=True)
    return whole.reshape(-1, *inside)


def exchange_by_chip(shard, groups, order, split_dim, concat_dim):
    devices = lax.axis_size(groups[0]) * lax.axis_size(groups[1])
    pieces = cut_along(shard, split_dim, devices)
    return joined_along(exchange_in_order(pieces, groups, order), concat_dim)


def side_by_side(arrays, axis, dim, along):
    widths = [a.shape[along] for a in arrays]
    both = jnp.concatenate(arrays, axis=along)
    whole = lax.all_gather(both, axis, axis=dim, tiled=True)
    return tuple(jnp.split(whole, [sum(widths[:k]) for k in range(1, len(widths))], axis=along))


def normalize(rows, gain):
    values = rows.astype(jnp.float32)
    scaled = values * lax.rsqrt(jnp.mean(values * values, axis=-1, keepdims=True) + EPSILON)
    return (scaled * gain).astype(jnp.bfloat16)


def turn(values, cosine, sine):
    first, second = jnp.split(values, 2, axis=-1)
    cosine = cosine[:, None, :]
    sine = sine[:, None, :]
    return jnp.concatenate(
        [first * cosine - second * sine, second * cosine + first * sine], axis=-1
    )


def axial_rope(values, places):
    quarter = values.shape[-1] // 4
    frequency = BASE ** (-jnp.arange(quarter, dtype=jnp.float32) / quarter)
    row_angle = (places // GRID_W).astype(jnp.float32)[:, None] * frequency[None, :]
    column_angle = (places % GRID_W).astype(jnp.float32)[:, None] * frequency[None, :]
    row_part, column_part = jnp.split(values, 2, axis=-1)
    return jnp.concatenate(
        [
            turn(row_part, jnp.cos(row_angle), jnp.sin(row_angle)),
            turn(column_part, jnp.cos(column_angle), jnp.sin(column_angle)),
        ],
        axis=-1,
    )


def activate(gate, up):
    capped = jnp.minimum(gate, LIMIT)
    bounded = jnp.clip(up, -LIMIT, LIMIT)
    return (capped * jax.nn.sigmoid(SLOPE * capped) * (bounded + 1.0)).astype(jnp.bfloat16)


def add_product(piece, weight):
    return jnp.dot(piece, weight, preferred_element_type=jnp.float32)


def shards(
    mixer_input,
    mixer_gain,
    query_weight,
    key_weight,
    value_weight,
    output_weight,
    sink_logit,
    expert_input,
    expert_gain,
    routes,
    route_logits,
    gate_weight,
    up_weight,
    down_weight,
):
    tokens = mixer_input.shape[0]
    query_heads = query_weight.shape[1] // HEAD_DIM
    key_heads = key_weight.shape[1] // HEAD_DIM
    group = query_heads // key_heads
    blocks = tokens // WINDOW
    offset = lax.axis_index(EP) * tokens
    length = lax.axis_size(EP) * tokens
    places = offset + jnp.arange(tokens, dtype=jnp.int32)
    normed = normalize(mixer_input, mixer_gain)
    query = jnp.dot(normed, query_weight, preferred_element_type=jnp.float32).reshape(
        tokens, query_heads, HEAD_DIM
    )
    query = (
        axial_rope(query, places)
        .astype(jnp.bfloat16)
        .reshape(blocks, WINDOW, key_heads, group, HEAD_DIM)
    )
    keys = jnp.dot(normed, key_weight, preferred_element_type=jnp.float32).reshape(
        tokens, key_heads, HEAD_DIM
    )
    keys = axial_rope(keys, places).astype(jnp.bfloat16).reshape(tokens, key_heads * HEAD_DIM)
    values = jnp.dot(normed, value_weight, preferred_element_type=jnp.float32).astype(jnp.bfloat16)
    stacked = jnp.concatenate([keys, values], axis=1)
    widened = extended(stacked, ((EP, 0),), WINDOW)
    framed = widened.reshape(blocks + 2, WINDOW, 2, key_heads, HEAD_DIM)
    nearby = jnp.concatenate([framed[:-2], framed[1:-1], framed[2:]], axis=1)
    scores = jnp.einsum(
        "nqgrd,nkgd->ngrqk", query, nearby[:, :, 0], preferred_element_type=jnp.float32
    ) * HEAD_DIM ** (-0.5)
    query_place = places.reshape(blocks, WINDOW)
    key_place = (
        offset
        + (jnp.arange(blocks, dtype=jnp.int32)[:, None] - 1) * WINDOW
        + jnp.arange(3 * WINDOW, dtype=jnp.int32)[None, :]
    )
    allowed = (
        (jnp.abs(query_place[:, :, None] - key_place[:, None, :]) <= WINDOW)
        & (key_place[:, None, :] >= 0)
        & (key_place[:, None, :] < length)
    )
    scores = jnp.where(allowed[:, None, None], scores, -1e30)
    sinks = sink_logit.reshape(key_heads, group)[None, :, :, None]
    top = jnp.maximum(jnp.max(scores, axis=-1), sinks)
    weights = jnp.exp(scores - top[..., None])
    denominator = jnp.sum(weights, axis=-1) + jnp.exp(sinks - top)
    shares = (weights / denominator[..., None]).astype(jnp.bfloat16)
    mixed = jnp.einsum(
        "ngrqk,nkgd->nqgrd", shares, nearby[:, :, 1], preferred_element_type=jnp.float32
    )
    mixed = mixed.astype(jnp.bfloat16).reshape(tokens, query_heads * HEAD_DIM)
    experts = lax.axis_size(EP)
    rows_here = expert_input.shape[0]
    capacity = 2 * rows_here * TOP_K // experts
    expert_normed = normalize(expert_input, expert_gain)
    chances = jax.nn.softmax(route_logits, axis=-1)
    chosen = routes.reshape(-1)
    marks = (chosen[:, None] == jnp.arange(experts, dtype=jnp.int32)[None, :]).astype(jnp.int32)
    earlier = jnp.sum((jnp.cumsum(marks, axis=0) - marks) * marks, axis=1)
    target = chosen * capacity + earlier
    source = (
        jnp.full((experts * capacity,), rows_here, jnp.int32)
        .at[target]
        .set(jnp.arange(chosen.shape[0], dtype=jnp.int32) // TOP_K)
    )
    padded = jnp.concatenate(
        [expert_normed, jnp.zeros((1, expert_normed.shape[1]), jnp.bfloat16)], axis=0
    )
    down_local = down_weight[0]
    gate_local = gate_weight[0]
    up_local = up_weight[0]
    width = padded.shape[1] // lax.axis_size("tp")
    own = lax.dynamic_slice_in_dim(padded, lax.axis_index("tp") * width, width, 1)
    outgoing = own[source].reshape(experts, capacity, width)
    received = lax.all_to_all(outgoing, EP, split_axis=0, concat_axis=0, tiled=True)
    flat = received.reshape(experts * capacity, width)
    head_piece, feature_piece = side_by_side((mixed, flat), "tp", 1, 0)
    mixer_total = add_product(head_piece, output_weight)
    gate = add_product(feature_piece, gate_local)
    up = add_product(feature_piece, up_local)
    hidden = activate(gate, up)
    result = add_product(lax.all_gather(hidden, "tp", axis=1, tiled=True), down_local)
    result = result.astype(jnp.bfloat16).reshape(experts, capacity, down_local.shape[1])
    returned = exchange_by_chip(result, ("ep_0", "ep_1"), (1, 0), 0, 0)
    mixer_output = mixer_total.astype(jnp.bfloat16)
    results = returned.reshape(experts * capacity, returned.shape[2])
    picked = results[target].astype(jnp.float32).reshape(rows_here, TOP_K, returned.shape[2])
    expert_output = jnp.sum(picked * chances[:, :, None], axis=1).astype(jnp.bfloat16)
    return (mixer_output, expert_output)


def solution(mesh):
    finer = Mesh(mesh.devices.reshape(16, 2, mesh.shape["tp"]), ("ep_0", "ep_1", "tp"))
    in_specs = (
        P(EP, None),
        P(),
        P(None, "tp"),
        P(None, "tp"),
        P(None, "tp"),
        P(None, "tp"),
        P("tp"),
        P(EP, None),
        P(),
        P(EP, None),
        P(EP, None),
        P(EP, None, "tp"),
        P(EP, None, "tp"),
        P(EP, None, "tp"),
    )
    out_specs = (P(EP, "tp"), P(EP, "tp"))
    return jax.shard_map(
        shards, mesh=finer, in_specs=in_specs, out_specs=out_specs, check_vma=False
    )
```

profile of v0, /device:TPU:32, one launch (start us, length us, event | category | flops | bytes accessed | tf_op | source)
XLA Modules:
  0.0 255.0 jit_solution(9797498149042853800)
XLA Ops:
  7.2 0.7 broadcast_multiply_fusion
  7.9 0.8 copy.46
  8.9 1.2 fusion.26
  10.4 1.2 reduce-window.6
  12.0 2.4 scatter_custom_fusion
  14.5 1.3 fusion.28
  15.8 4.3 %gather_fusion = bf16[1024,128]{1,0:T(8,128)(2,1)} fusion(bf16[129,128]{1,0:T(8,128)(2,1)S(1)} %pad_dynamic-slice_fusion, s32[1024]{0:T(1024)S(1)} %fusion.69), kind=kCustom, calls=%fused_computation | custom fusion | bytes 528384 | tf_op jit(solution)/shard_map/gather | solution.py:192
  20.1 15.5 %all-to-all-start = ((bf16[32,32,128]{2,1,0:T(8,128)(2,1)}), bf16[32,32,128]{2,1,0:T(8,128)(2,1)S(1)}, u32[]{:S(2)}, u32[]{:S(2)}) async-start(bf16[32,32,128]{2,1,0:T(8,128)(2,1)} %bitcast.20), calls=%async_computation | async-start | bytes 524288 | tf_op jit(solution)/shard_map/all_to_all | solution.py:193
  37.7 2.0 collective-permute-start.1
  39.7 2.3 collective-permute-start
  43.6 3.0 %collective-permute-done.1 = bf16[128,128]{0,1:T(8,128)(2,1)S(1)} collective-permute-done((bf16[128,128]{0,1:T(8,128)(2,1)S(1)}, bf16[128,128]{0,1:T(8,128)(2,1)S(1)}, u32[]{:S(2)}, u32[]{:S(2)}) %collective-permute-start.1) | collective-permute-done | bytes 32800 | tf_op jit(solution)/shard_map/ppermute | solution.py:26
  47.8 8.7 %all-to-all-done = bf16[32,32,128]{2,1,0:T(8,128)(2,1)S(1)} async-done(((bf16[32,32,128]{2,1,0:T(8,128)(2,1)}), bf16[32,32,128]{2,1,0:T(8,128)(2,1)S(1)}, u32[]{:S(2)}, u32[]{:S(2)}) %all-to-all-start) | async-done | bytes 262176 | tf_op jit(solution)/shard_map/all_to_all | solution.py:193
  56.6 0.7 pad_maximum_fusion
  57.4 71.7 %all-gather.3.cloned.1.call-done = bf16[1280,2048]{1,0:T(8,128)(2,1)} async-done(((bf16[1280,128]{1,0:T(8,128)(2,1)}), bf16[1280,2048]{1,0:T(8,128)(2,1)}) %all-gather.3.cloned.1.call-update) | async-done | bytes 5242896 | tf_op jit(solution)/shard_map/all_gather | solution.py:60
  129.1 3.6 %fusion.8 = f32[1024,128]{1,0:T(8,128)S(1)} fusion(bf16[1280,2048]{1,0:T(8,128)(2,1)} %all-gather.3.cloned.1.call-done, bf16[1,2048,128]{2,1,0:T(8,128)(2,1)S(1)} %copy-done), kind=kOutput, calls=%fused_computation.16 | convolution fusion | flops 537001984 | bytes 5242880 | tf_op jit(solution)/shard_map/dot_general | solution.py:101
  132.8 2.0 fusion.21
  134.8 71.7 %all-gather.5.cloned.1.call-done = bf16[1024,2048]{1,0:T(8,128)(2,1)} async-done(((bf16[1024,128]{1,0:T(8,128)(2,1)}), bf16[1024,2048]{1,0:T(8,128)(2,1)}) %all-gather.5.cloned.1.call-update) | async-done | bytes 4194320 | tf_op jit(solution)/shard_map/all_gather | solution.py:200
  206.6 3.4 %convolution_convert_fusion = bf16[1024,128]{1,0:T(8,128)(2,1)S(1)} fusion(bf16[1024,2048]{1,0:T(8,128)(2,1)} %all-gather.5.cloned.1.call-done, bf16[1,2048,128]{2,1,0:T(8,128)(2,1)S(1)} %copy-done.7), kind=kOutput, calls=%fused_computation.22 | convolution fusion | flops 537001984 | bytes 4980736 | tf_op jit(solution)/shard_map/dot_general | solution.py:101
  210.1 4.1 %all_to_all.15 = bf16[16,2,1,32,128]{4,3,0,2,1:T(8,128)(2,1)S(1)} all-to-all(bf16[16,2,1,32,128]{4,3,0,2,1:T(8,128)(2,1)S(1)} %copy.50), channel_id=1, replica_groups=mesh['ep_0'=16,'ep_1'=2,'tp'=16] {'ep_1'}, dimensions={1} | all-to-all | bytes 524288 | tf_op jit(solution)/shard_map/all_to_all | solution.py:47
  214.9 12.7 %all-to-all-start.2 = ((bf16[16,2,1,32,128]{4,3,1,2,0:T(8,128)(2,1)}), bf16[16,2,1,32,128]{4,3,1,2,0:T(8,128)(2,1)S(1)}, u32[]{:S(2)}, u32[]{:S(2)}) async-start(bf16[16,2,1,32,128]{4,3,1,2,0:T(8,128)(2,1)} %copy.51), calls=%async_computation.2 | async-start | bytes 524288 | tf_op jit(solution)/shard_map/all_to_all | solution.py:47
  227.7 2.3 convolution_convert_fusion.1
  230.0 15.9 %all-to-all-done.2 = bf16[16,2,1,32,128]{4,3,1,2,0:T(8,128)(2,1)S(1)} async-done(((bf16[16,2,1,32,128]{4,3,1,2,0:T(8,128)(2,1)}), bf16[16,2,1,32,128]{4,3,1,2,0:T(8,128)(2,1)S(1)}, u32[]{:S(2)}, u32[]{:S(2)}) %all-to-all-start.2) | async-done | bytes 262176 | tf_op jit(solution)/shard_map/all_to_all | solution.py:47
  245.9 1.3 gather_fusion.1
  247.2 0.9 fusion.37
  (87 shorter events, 6.7 us)
Async XLA Ops:
  7.2 121.9 %copy-start = (bf16[1,2048,128]{2,1,0:T(8,128)(2,1)S(1)}, bf16[1,2048,128]{2,1,0:T(8,128)(2,1)}, u32[]{:S(2)}) copy-start(bf16[1,2048,128]{2,1,0:T(8,128)(2,1)} %param.25) | copy-start | bytes 1572868
  14.4 21.2 %copy-start.1 = (bf16[256,2048]{1,0:T(8,128)(2,1)S(1)}, bf16[256,2048]{1,0:T(8,128)(2,1)}, u32[]{:S(2)}) copy-start(bf16[256,2048]{1,0:T(8,128)(2,1)} %param.14) | copy-start | bytes 3145732
  15.8 20.2 %copy-start.9 = (bf16[2048,64]{0,1:T(8,128)(2,1)S(1)}, bf16[2048,64]{0,1:T(8,128)(2,1)}, u32[]{:S(2)}) copy-start(bf16[2048,64]{0,1:T(8,128)(2,1)} %param.17) | copy-start | bytes 786436
  15.8 20.2 %copy-start.11 = (f32[2048]{0:T(1024)S(1)}, f32[2048]{0:T(1024)}, u32[]{:S(2)}) copy-start(f32[2048]{0:T(1024)} %param.15) | copy-start | bytes 24580
  20.1 17.0 %copy-start.10 = (bf16[2048,64]{0,1:T(8,128)(2,1)S(1)}, bf16[2048,64]{0,1:T(8,128)(2,1)}, u32[]{:S(2)}) copy-start(bf16[2048,64]{0,1:T(8,128)(2,1)} %param.18) | copy-start | bytes 786436
  20.1 36.5 %all-to-all-start = ((bf16[32,32,128]{2,1,0:T(8,128)(2,1)}), bf16[32,32,128]{2,1,0:T(8,128)(2,1)S(1)}, u32[]{:S(2)}, u32[]{:S(2)}) async-start(bf16[32,32,128]{2,1,0:T(8,128)(2,1)} %bitcast.20), calls=%async_computation | async-start | bytes 524288 | tf_op jit(solution)/shard_map/all_to_all | solution.py:193
  35.6 93.5 %all-gather.3.cloned.1.call-start = ((), (), s32[]{:S(2)}) async-start(), calls=%async_computation.3 | async-start | bytes 5570560 | tf_op jit(solution)/shard_map/all_gather | solution.py:60
  36.0 6.4 %copy-start.5 = (bf16[2048,128]{1,0:T(8,128)(2,1)S(1)}, bf16[2048,128]{1,0:T(8,128)(2,1)}, u32[]{:S(2)}) copy-start(bf16[2048,128]{1,0:T(8,128)(2,1)} %param.16) | copy-start | bytes 1572868
  37.7 8.9 %collective-permute-start.1 = (bf16[128,128]{0,1:T(8,128)(2,1)S(1)}, bf16[128,128]{0,1:T(8,128)(2,1)S(1)}, u32[]{:S(2)}, u32[]{:S(2)}) collective-permute-start(bf16[128,128]{0,1:T(8,128)(2,1)S(1)} %get-tuple-element.10), channel_id=1, source_target_pairs={{16,0},{32,16},{48,32},{64,48},{80,64},{96,80},{112,96},{128,112},... | collective-permute-start | bytes 98312 | tf_op jit(solution)/shard_map/ppermute | solution.py:26
  39.7 6.9 %collective-permute-start = (bf16[128,128]{0,1:T(8,128)(2,1)S(1)}, bf16[128,128]{0,1:T(8,128)(2,1)S(1)}, u32[]{:S(2)}, u32[]{:S(2)}) collective-permute-start(bf16[128,128]{0,1:T(8,128)(2,1)S(1)} %get-tuple-element.11), channel_id=1, source_target_pairs={{0,16},{16,32},{32,48},{48,64},{64,80},{80,96},{96,112},{112,128},... | collective-permute-start | bytes 98312 | tf_op jit(solution)/shard_map/ppermute | solution.py:25
  42.4 4.7 %copy-start.3 = (f32[2]{0:T(128)S(1)}, f32[2]{0:T(128)}, u32[]{:S(2)}) copy-start(f32[2]{0:T(128)} %param.20) | copy-start | bytes 28
  57.3 75.3 %copy-start.6 = (bf16[1,2048,128]{2,1,0:T(8,128)(2,1)S(1)}, bf16[1,2048,128]{2,1,0:T(8,128)(2,1)}, u32[]{:S(2)}) copy-start(bf16[1,2048,128]{2,1,0:T(8,128)(2,1)} %param.26) | copy-start | bytes 1572868
  57.4 149.2 %all-gather.5.cloned.1.call-start = ((), (), s32[]{:S(2)}) async-start(), calls=%async_computation.4 | async-start | bytes 4456448 | tf_op jit(solution)/shard_map/all_gather | solution.py:200
  129.1 3.7 %copy-start.4 = (bf16[1280,2048]{1,0:T(8,128)(2,1)S(1)}, bf16[1280,2048]{1,0:T(8,128)(2,1)}, u32[]{:S(2)}) copy-start(bf16[1280,2048]{1,0:T(8,128)(2,1)} %all-gather.3.cloned.1.call-done) | copy-start | bytes 15728644
  132.8 73.7 %copy-start.7 = (bf16[1,2048,128]{2,1,0:T(8,128)(2,1)S(1)}, bf16[1,2048,128]{2,1,0:T(8,128)(2,1)}, u32[]{:S(2)}) copy-start(bf16[1,2048,128]{2,1,0:T(8,128)(2,1)} %param.27) | copy-start | bytes 1572868
  210.0 17.5 %copy-start.2 = (f32[128,4]{0,1:T(4,128)S(1)}, f32[128,4]{0,1:T(4,128)}, u32[]{:S(2)}) copy-start(f32[128,4]{0,1:T(4,128)} %param.24) | copy-start | bytes 6148
  210.0 17.7 %copy-start.8 = (bf16[2048,128]{1,0:T(8,128)(2,1)S(1)}, bf16[2048,128]{1,0:T(8,128)(2,1)}, u32[]{:S(2)}) copy-start(bf16[2048,128]{1,0:T(8,128)(2,1)} %param.19) | copy-start | bytes 1572868
  214.9 31.0 %all-to-all-start.2 = ((bf16[16,2,1,32,128]{4,3,1,2,0:T(8,128)(2,1)}), bf16[16,2,1,32,128]{4,3,1,2,0:T(8,128)(2,1)S(1)}, u32[]{:S(2)}, u32[]{:S(2)}) async-start(bf16[16,2,1,32,128]{4,3,1,2,0:T(8,128)(2,1)} %copy.51), calls=%async_computation.2 | async-start | bytes 524288 | tf_op jit(solution)/shard_map/all_to_all | solution.py:47
Sparse Core Ops, SparseCore 0:
  57.5 71.5 all-gather.2
  134.9 71.5 all-gather.4
where the time goes:
time: 255 us
  waiting for transfers between devices  171 us (67%)
  starting transfers between devices  32.6 us (13%)
  between operations  14.5 us (6%)
  matrix products  13.4 us (5%)
  local copies, waits for them, and re-layouts  11 us (4%)
  other arithmetic  8.38 us (3%)
  blocking collectives  4.08 us (2%)
    all_gather x1, waiting for transfers between devices, shards(): lax.all_gather(hidden, 'tp', axis=1, tiled=True)  71.7 us
    all_gather x1, waiting for transfers between devices, side_by_side(): whole = lax.all_gather(both, axis, axis=dim, tiled=True)  71.7 us
    all_to_all x1, waiting for transfers between devices, exchange_in_order(): whole = lax.all_to_all(whole, axes[k], k, k, tiled=True)  15.9 us
    all_to_all x1, starting transfers between devices, shards(): lax.all_to_all(outgoing, EP, split_axis=0, concat_axis=0, tiled=True)  15.5 us
    all_to_all x1, starting transfers between devices, exchange_in_order(): whole = lax.all_to_all(whole, axes[k], k, k, tiled=True)  12.7 us
    dot_general x4, matrix products, add_product(): return jnp.dot(piece, weight, preferred_element_type=jnp.float32)  11.3 us
    all_to_all x1, waiting for transfers between devices, shards(): lax.all_to_all(outgoing, EP, split_axis=0, concat_axis=0, tiled=True)  8.72 us
  transfers between devices with their start and end apart: 6, of which 5 were waited for; matrix products, arithmetic and copies ran while one was open for 3% of the time, Pallas kernels for 0%

commit v1 on v0

--- a/solution.py
+++ b/solution.py
@@ -13,6 +13,14 @@
 LIMIT = 7.0
 SLOPE = 1.702
 BASE = 10000.0
+
+
+def gather_from_all(shard, axis, dim):
+    devices = lax.axis_size(axis)
+    repeats = [devices if d == dim else 1 for d in range(shard.ndim)]
+    return lax.all_to_all(
+        jnp.tile(shard, repeats), axis, split_axis=dim, concat_axis=dim, tiled=True
+    )
 
 
 def extended(shard, sides, width):
@@ -197,7 +205,7 @@
     gate = add_product(feature_piece, gate_local)
     up = add_product(feature_piece, up_local)
     hidden = activate(gate, up)
-    result = add_product(lax.all_gather(hidden, "tp", axis=1, tiled=True), down_local)
+    result = add_product(gather_from_all(hidden, "tp", 1), down_local)
     result = result.astype(jnp.bfloat16).reshape(experts, capacity, down_local.shape[1])
     returned = exchange_by_chip(result, ("ep_0", "ep_1"), (1, 0), 0, 0)
     mixer_output = mixer_total.astype(jnp.bfloat16)

time: 255 us -> 246 us (0.965)
  the two profiles are of different devices: /device:TPU:32 before, /device:TPU:2 now
where the time goes in v1:
time: 246 us; the launch traced here: 245 us
  waiting for transfers between devices  99.4 us (40%)
  blocking collectives  59.8 us (24%)
  starting transfers between devices  32.1 us (13%)
  local copies, waits for them, and re-layouts  18.3 us (7%)
  between operations  14.5 us (6%)
  matrix products  12.9 us (5%)
  other arithmetic  8.36 us (3%)
    all_gather x1, waiting for transfers between devices, side_by_side(): whole = lax.all_gather(both, axis, axis=dim, tiled=True)  69.7 us
    all_to_all x1, blocking collectives, gather_from_all(): lax.all_to_all(jnp.tile(shard, repeats), axis, split_axis=dim, concat_axi...  55.8 us
    all_to_all x1, waiting for transfers between devices, exchange_in_order(): whole = lax.all_to_all(whole, axes[k], k, k, tiled=True)  16 us
    all_to_all x1, starting transfers between devices, shards(): lax.all_to_all(outgoing, EP, split_axis=0, concat_axis=0, tiled=True)  15.5 us
    all_to_all x1, waiting for transfers between devices, shards(): lax.all_to_all(outgoing, EP, split_axis=0, concat_axis=0, tiled=True)  13.6 us
    all_to_all x1, starting transfers between devices, exchange_in_order(): whole = lax.all_to_all(whole, axes[k], k, k, tiled=True)  12.3 us
    dot_general x4, matrix products, add_product(): return jnp.dot(piece, weight, preferred_element_type=jnp.float32)  10.7 us
    all_to_all x1, local copies, waits for them, and re-layouts, gather_from_all(): lax.all_to_all(jnp.tile(shard, repeats), axis, split_axis=dim, concat_axi...  6.51 us
  transfers between devices with their start and end apart: 5, of which 3 were waited for; matrix products, arithmetic and copies ran while one was open for 3% of the time, Pallas kernels for 0%

profile of v1, /device:TPU:2, one launch (start us, length us, event | category | flops | bytes accessed | tf_op | source)
XLA Modules:
  0.0 245.3 jit_solution(1807772073622336707)
XLA Ops:
  7.2 0.8 broadcast_multiply_fusion
  8.0 0.8 copy.63
  9.0 1.2 fusion.26
  10.5 1.2 reduce-window.6
  12.1 2.4 scatter_custom_fusion
  14.6 1.2 fusion.28
  15.8 4.3 %gather_fusion = bf16[1024,128]{1,0:T(8,128)(2,1)} fusion(bf16[129,128]{1,0:T(8,128)(2,1)S(1)} %pad_dynamic-slice_fusion, s32[1024]{0:T(1024)S(1)} %fusion.69), kind=kCustom, calls=%fused_computation | custom fusion | bytes 528384 | tf_op jit(solution)/shard_map/gather | solution.py:200
  20.1 15.5 %all-to-all-start = ((bf16[32,32,128]{2,1,0:T(8,128)(2,1)}), bf16[32,32,128]{2,1,0:T(8,128)(2,1)S(1)}, u32[]{:S(2)}, u32[]{:S(2)}) async-start(bf16[32,32,128]{2,1,0:T(8,128)(2,1)} %bitcast.20), calls=%async_computation | async-start | bytes 524288 | tf_op jit(solution)/shard_map/all_to_all | solution.py:201
  37.6 1.3 collective-permute-start.1
  38.9 3.0 %collective-permute-start = (bf16[128,128]{0,1:T(8,128)(2,1)S(1)}, bf16[128,128]{0,1:T(8,128)(2,1)S(1)}, u32[]{:S(2)}, u32[]{:S(2)}) collective-permute-start(bf16[128,128]{0,1:T(8,128)(2,1)S(1)} %get-tuple-element.11), channel_id=1, source_target_pairs={{0,16},{16,32},{32,48},{48,64},{64,80},{80,96},{96,112},{112,128},... | collective-permute-start | bytes 98312 | tf_op jit(solution)/shard_map/ppermute | solution.py:33
  44.9 13.6 %all-to-all-done = bf16[32,32,128]{2,1,0:T(8,128)(2,1)S(1)} async-done(((bf16[32,32,128]{2,1,0:T(8,128)(2,1)}), bf16[32,32,128]{2,1,0:T(8,128)(2,1)S(1)}, u32[]{:S(2)}, u32[]{:S(2)}) %all-to-all-start) | async-done | bytes 262176 | tf_op jit(solution)/shard_map/all_to_all | solution.py:201
  59.3 69.7 %all-gather.2.cloned.1.call-done = bf16[1280,2048]{1,0:T(8,128)(2,1)} async-done(((bf16[1280,128]{1,0:T(8,128)(2,1)}), bf16[1280,2048]{1,0:T(8,128)(2,1)}) %all-gather.2.cloned.1.call-update) | async-done | bytes 5242896 | tf_op jit(solution)/shard_map/all_gather | solution.py:68
  129.0 3.6 %fusion.8 = f32[1024,128]{1,0:T(8,128)S(1)} fusion(bf16[1280,2048]{1,0:T(8,128)(2,1)} %all-gather.2.cloned.1.call-done, bf16[1,2048,128]{2,1,0:T(8,128)(2,1)S(1)} %copy-done), kind=kOutput, calls=%fused_computation.16 | convolution fusion | flops 537001984 | bytes 5242880 | tf_op jit(solution)/shard_map/dot_general | solution.py:109
  132.7 1.3 fusion.21
  134.0 0.8 tile.2
  134.8 55.8 %all_to_all.24 = bf16[1024,16,128]{2,0,1:T(8,128)(2,1)} all-to-all(bf16[1024,16,128]{2,0,1:T(8,128)(2,1)S(1)} %tile.2), channel_id=1, replica_groups=mesh['ep_0'=16,'ep_1'=2,'tp'=16] {'tp'}, dimensions={1} | all-to-all | bytes 8388608 | tf_op jit(solution)/shard_map/all_to_all | solution.py:21
  190.6 6.5 %copy.67 = bf16[1024,16,128]{0,2,1:T(8,128)(2,1)} copy(bf16[1024,16,128]{2,0,1:T(8,128)(2,1)} %all_to_all.24) | data formatting | bytes 8388608 | tf_op jit(solution)/shard_map/all_to_all | solution.py:21
  197.1 3.6 %convolution_convert_fusion = bf16[1024,128]{1,0:T(8,128)(2,1)S(1)} fusion(bf16[1024,2048]{0,1:T(8,128)(2,1)} %bitcast.111, bf16[1,2048,128]{2,1,0:T(8,128)(2,1)S(1)} %copy-done.7), kind=kOutput, calls=%fused_computation.22 | convolution fusion | flops 537001984 | bytes 4980736 | tf_op jit(solution)/shard_map/dot_general | solution.py:109
  200.7 3.9 %all_to_all.25 = bf16[16,2,1,32,128]{4,3,0,2,1:T(8,128)(2,1)S(1)} all-to-all(bf16[16,2,1,32,128]{4,3,0,2,1:T(8,128)(2,1)S(1)} %copy.68), channel_id=1, replica_groups=mesh['ep_0'=16,'ep_1'=2,'tp'=16] {'ep_1'}, dimensions={1} | all-to-all | bytes 524288 | tf_op jit(solution)/shard_map/all_to_all | solution.py:55
  205.4 12.3 %all-to-all-start.3 = ((bf16[16,2,1,32,128]{4,3,1,2,0:T(8,128)(2,1)}), bf16[16,2,1,32,128]{4,3,1,2,0:T(8,128)(2,1)S(1)}, u32[]{:S(2)}, u32[]{:S(2)}) async-start(bf16[16,2,1,32,128]{4,3,1,2,0:T(8,128)(2,1)} %copy.69), calls=%async_computation.3 | async-start | bytes 524288 | tf_op jit(solution)/shard_map/all_to_all | solution.py:55
  217.9 2.3 convolution_convert_fusion.1
  220.2 16.0 %all-to-all-done.3 = bf16[16,2,1,32,128]{4,3,1,2,0:T(8,128)(2,1)S(1)} async-done(((bf16[16,2,1,32,128]{4,3,1,2,0:T(8,128)(2,1)}), bf16[16,2,1,32,128]{4,3,1,2,0:T(8,128)(2,1)S(1)}, u32[]{:S(2)}, u32[]{:S(2)}) %all-to-all-start.3) | async-done | bytes 262176 | tf_op jit(solution)/shard_map/all_to_all | solution.py:55
  236.2 1.3 gather_fusion.1
  237.5 0.9 fusion.37
  (87 shorter events, 7.4 us)
Async XLA Ops:
  7.2 121.8 %copy-start = (bf16[1,2048,128]{2,1,0:T(8,128)(2,1)S(1)}, bf16[1,2048,128]{2,1,0:T(8,128)(2,1)}, u32[]{:S(2)}) copy-start(bf16[1,2048,128]{2,1,0:T(8,128)(2,1)} %param.25) | copy-start | bytes 1572868
  7.2 28.5 %copy-start.1 = (bf16[256,2048]{1,0:T(8,128)(2,1)S(1)}, bf16[256,2048]{1,0:T(8,128)(2,1)}, u32[]{:S(2)}) copy-start(bf16[256,2048]{1,0:T(8,128)(2,1)} %param.14) | copy-start | bytes 3145732
  7.2 28.8 %copy-start.11 = (f32[2048]{0:T(1024)S(1)}, f32[2048]{0:T(1024)}, u32[]{:S(2)}) copy-start(f32[2048]{0:T(1024)} %param.15) | copy-start | bytes 24580
  7.2 28.8 %copy-start.9 = (bf16[2048,64]{0,1:T(8,128)(2,1)S(1)}, bf16[2048,64]{0,1:T(8,128)(2,1)}, u32[]{:S(2)}) copy-start(bf16[2048,64]{0,1:T(8,128)(2,1)} %param.17) | copy-start | bytes 786436
  10.3 26.8 %copy-start.10 = (bf16[2048,64]{0,1:T(8,128)(2,1)S(1)}, bf16[2048,64]{0,1:T(8,128)(2,1)}, u32[]{:S(2)}) copy-start(bf16[2048,64]{0,1:T(8,128)(2,1)} %param.18) | copy-start | bytes 786436
  15.8 26.5 %copy-start.5 = (bf16[2048,128]{1,0:T(8,128)(2,1)S(1)}, bf16[2048,128]{1,0:T(8,128)(2,1)}, u32[]{:S(2)}) copy-start(bf16[2048,128]{1,0:T(8,128)(2,1)} %param.16) | copy-start | bytes 1572868
  20.1 38.4 %all-to-all-start = ((bf16[32,32,128]{2,1,0:T(8,128)(2,1)}), bf16[32,32,128]{2,1,0:T(8,128)(2,1)S(1)}, u32[]{:S(2)}, u32[]{:S(2)}) async-start(bf16[32,32,128]{2,1,0:T(8,128)(2,1)} %bitcast.20), calls=%async_computation | async-start | bytes 524288 | tf_op jit(solution)/shard_map/all_to_all | solution.py:201
  35.6 93.4 %all-gather.2.cloned.1.call-start = ((), (), s32[]{:S(2)}) async-start(), calls=%async_computation.4 | async-start | bytes 5570560 | tf_op jit(solution)/shard_map/all_gather | solution.py:68
  36.5 7.5 %copy-start.3 = (f32[2]{0:T(128)S(1)}, f32[2]{0:T(128)}, u32[]{:S(2)}) copy-start(f32[2]{0:T(128)} %param.20) | copy-start | bytes 28
  37.6 5.9 %collective-permute-start.1 = (bf16[128,128]{0,1:T(8,128)(2,1)S(1)}, bf16[128,128]{0,1:T(8,128)(2,1)S(1)}, u32[]{:S(2)}, u32[]{:S(2)}) collective-permute-start(bf16[128,128]{0,1:T(8,128)(2,1)S(1)} %get-tuple-element.10), channel_id=1, source_target_pairs={{16,0},{32,16},{48,32},{64,48},{80,64},{96,80},{112,96},{128,112},... | collective-permute-start | bytes 98312 | tf_op jit(solution)/shard_map/ppermute | solution.py:34
  38.9 4.6 %collective-permute-start = (bf16[128,128]{0,1:T(8,128)(2,1)S(1)}, bf16[128,128]{0,1:T(8,128)(2,1)S(1)}, u32[]{:S(2)}, u32[]{:S(2)}) collective-permute-start(bf16[128,128]{0,1:T(8,128)(2,1)S(1)} %get-tuple-element.11), channel_id=1, source_target_pairs={{0,16},{16,32},{32,48},{48,64},{64,80},{80,96},{96,112},{112,128},... | collective-permute-start | bytes 98312 | tf_op jit(solution)/shard_map/ppermute | solution.py:33
  59.2 73.3 %copy-start.6 = (bf16[1,2048,128]{2,1,0:T(8,128)(2,1)S(1)}, bf16[1,2048,128]{2,1,0:T(8,128)(2,1)}, u32[]{:S(2)}) copy-start(bf16[1,2048,128]{2,1,0:T(8,128)(2,1)} %param.26) | copy-start | bytes 1572868
  129.0 3.7 %copy-start.4 = (bf16[1280,2048]{1,0:T(8,128)(2,1)S(1)}, bf16[1280,2048]{1,0:T(8,128)(2,1)}, u32[]{:S(2)}) copy-start(bf16[1280,2048]{1,0:T(8,128)(2,1)} %all-gather.2.cloned.1.call-done) | copy-start | bytes 15728644
  190.6 6.5 %copy-start.7 = (bf16[1,2048,128]{2,1,0:T(8,128)(2,1)S(1)}, bf16[1,2048,128]{2,1,0:T(8,128)(2,1)}, u32[]{:S(2)}) copy-start(bf16[1,2048,128]{2,1,0:T(8,128)(2,1)} %param.27) | copy-start | bytes 1572868
  197.1 20.6 %copy-start.2 = (f32[128,4]{0,1:T(4,128)S(1)}, f32[128,4]{0,1:T(4,128)}, u32[]{:S(2)}) copy-start(f32[128,4]{0,1:T(4,128)} %param.24) | copy-start | bytes 6148
  197.1 20.8 %copy-start.8 = (bf16[2048,128]{1,0:T(8,128)(2,1)S(1)}, bf16[2048,128]{1,0:T(8,128)(2,1)}, u32[]{:S(2)}) copy-start(bf16[2048,128]{1,0:T(8,128)(2,1)} %param.19) | copy-start | bytes 1572868
  205.4 30.8 %all-to-all-start.3 = ((bf16[16,2,1,32,128]{4,3,1,2,0:T(8,128)(2,1)}), bf16[16,2,1,32,128]{4,3,1,2,0:T(8,128)(2,1)S(1)}, u32[]{:S(2)}, u32[]{:S(2)}) async-start(bf16[16,2,1,32,128]{4,3,1,2,0:T(8,128)(2,1)} %copy.69), calls=%async_computation.3 | async-start | bytes 524288 | tf_op jit(solution)/shard_map/all_to_all | solution.py:55
Sparse Core Ops, SparseCore 0:
  59.4 69.5 all-gather.1
